TPU v7x, 32 devices: a whole 2x2x4 slice. The times are simulated.
32 devices in a mesh: grp: 2 (over y), ep: 4 (over z), tp: 4 (over x, core).
Axes of the slice: x: 2, y: 2, z: 4, core: 2. Of those that a mesh axis runs over, the one named last changes fastest.
Arguments:
- queries: bfloat16 [1024, 1024], P(('grp', 'ep'), 'tp'), parts along dimension 0, may hold values from -6 to 6
- keys: bfloat16 [1024, 1024], P(('grp', 'ep'), 'tp'), parts along dimension 0, may hold values from -6 to 6
- values: bfloat16 [1024, 1024], P(('grp', 'ep'), 'tp'), parts along dimension 0, may hold values from -6 to 6
- lambdas: float32 [8], P('tp'), may hold values from 0.3 to 0.8
- head_gain: float32 [128], replicated, may hold values from 0.1 to 1.9
- tokens: bfloat16 [2048, 1536], P(('grp', 'ep')), parts along dimension 0, may hold values from -6 to 6
- route_ids: int32 [2048, 2], P(('grp', 'ep')), parts along dimension 0, may hold values from 0 to 3, all different within a row; in each aligned block of 256 rows (0 to 255, 256 to 511, ...) at most 256 rows name the same one
- route_weights: float32 [2048, 2], P(('grp', 'ep')), parts along dimension 0, may hold values from 0.2 to 1
- moe_gain: float32 [1536], replicated, may hold values from 0.1 to 1.9
- w_gate: bfloat16 [4, 1536, 3072], P('ep', None, 'tp'), may hold values from -0.15625 to 0.15625
- w_up: bfloat16 [4, 1536, 3072], P('ep', None, 'tp'), may hold values from -0.15625 to 0.15625
- w_down: bfloat16 [4, 3072, 1536], P('ep', 'tp'), may hold values from -0.109375 to 0.109375
Outputs:
- heads_out: bfloat16 [1024, 1024], P(('grp', 'ep'), 'tp'), parts along dimension 0
- expert_out: bfloat16 [2048, 1536], P(('grp', 'ep'), 'tp'), parts along dimension 0
There are 2 independent parts, one for each index of `grp`. A program takes and returns all parts, laid end to end along the dimension named above; an argument that names none is the same for every part. Nothing has to cross between parts.
Inputs may be any that keep to these rules, and one draw needn't show every extreme that they name: `route_ids`: each row names 2 different experts. In the 256 rows of one device no expert is named more than 256 times, and in every draw some device names some expert exactly 256 times.
All inputs are finite; a program needn't handle non-finite values.
Results may differ from a plain program's by a relative error of at most 0.015.
Values may be sent and summed in bfloat16 or wider, within the bound.
A program may use at most 64 MiB of HBM per device.

v0:
```python
import jax
import jax.numpy as jnp
from jax import lax
from jax.sharding import PartitionSpec as P


def attend(queries, keys, values, lambdas, head_gain):
    row_count = queries.shape[0]
    head_count = lambdas.shape[0]
    head_dim = queries.shape[1] // (2 * head_count)
    value_dim = values.shape[1] // head_count
    query_parts = queries.reshape(row_count, head_count, 2, head_dim)
    score_scale = head_dim ** (-0.5)
    running = jnp.full((head_count, 2, row_count), -1e30, jnp.float32)
    key_piece = lax.all_gather(keys, "ep", axis=0, tiled=True)
    value_piece = lax.all_gather(values, "ep", axis=0, tiled=True)
    count = key_piece.shape[0]
    key_parts = key_piece.reshape(count, head_count, 2, head_dim)
    value_parts = value_piece.reshape(count, head_count, value_dim)
    scores = (
        jnp.einsum("qhcd,khcd->hcqk", query_parts, key_parts, preferred_element_type=jnp.float32)
        * score_scale
    )
    newest = jnp.maximum(running, jnp.max(scores, axis=-1))
    weights_now = jnp.exp(scores - newest[..., None])
    totals = jnp.sum(weights_now, axis=-1)
    sums = jnp.einsum(
        "hcqk,khe->hcqe",
        weights_now.astype(jnp.bfloat16),
        value_parts,
        preferred_element_type=jnp.float32,
    )
    running, totals, sums = (newest, totals, sums)
    means = sums / totals[..., None]
    mixed = means[:, 0] - lambdas[:, None, None] * means[:, 1]
    scaled = mixed * lax.rsqrt(jnp.mean(mixed * mixed, axis=-1, keepdims=True) + 1e-06) * head_gain
    return (
        jnp.transpose(scaled, (1, 0, 2))
        .reshape(row_count, head_count * value_dim)
        .astype(jnp.bfloat16)
    )


def experts(tokens, route_ids, route_weights, moe_gain, w_gate, w_up, w_down):
    row_count, width = tokens.shape
    top_count = route_ids.shape[1]
    ep_size = lax.axis_size("ep")
    tp_size = lax.axis_size("tp")
    expert_count = w_gate.shape[0] * ep_size
    capacity = 2 * row_count * top_count // expert_count
    token_float = tokens.astype(jnp.float32)
    normed = (
        token_float
        * lax.rsqrt(jnp.mean(token_float * token_float, axis=1, keepdims=True) + 1e-06)
        * moe_gain
    ).astype(jnp.bfloat16)
    flat_ids = route_ids.reshape(-1)
    onehot = (flat_ids[:, None] == jnp.arange(expert_count, dtype=jnp.int32)[None, :]).astype(
        jnp.int32
    )
    earlier = jnp.cumsum(onehot, axis=0) - onehot
    position = jnp.sum(earlier * onehot, axis=1)
    slot_index = flat_ids * capacity + position
    owners = (
        jnp.full((expert_count * capacity,), row_count, jnp.int32)
        .at[slot_index]
        .set(jnp.arange(row_count * top_count, dtype=jnp.int32) // top_count)
    )
    padded = jnp.concatenate([normed, jnp.zeros((1, width), jnp.bfloat16)], axis=0)
    outgoing = padded[owners].reshape(expert_count, capacity, width)
    gate_mat = w_gate[0]
    up_mat = w_up[0]
    down_mat = w_down[0]
    slice_width = width // tp_size
    own_columns = lax.dynamic_slice_in_dim(
        outgoing, lax.axis_index("tp") * slice_width, slice_width, 2
    )
    arrived = lax.all_to_all(own_columns, "ep", split_axis=0, concat_axis=0, tiled=True)
    piece = lax.all_gather(arrived, "tp", axis=2, tiled=True)
    gate = jnp.einsum("scd,df->scf", piece, gate_mat, preferred_element_type=jnp.float32)
    upward = jnp.einsum("scd,df->scf", piece, up_mat, preferred_element_type=jnp.float32)
    hidden = (jax.nn.silu(gate) * upward).astype(jnp.bfloat16)
    flat_hidden = hidden.reshape(-1, hidden.shape[2])
    summed = lax.psum_scatter(
        jnp.einsum("fd,sf->ds", down_mat, flat_hidden, preferred_element_type=jnp.float32).astype(
            jnp.bfloat16
        ),
        "tp",
        scatter_dimension=0,
        tiled=True,
    )
    back = lax.all_to_all(summed, "ep", split_axis=1, concat_axis=1, tiled=True)
    picked = (
        jnp.take(back, slot_index, axis=1).astype(jnp.float32).reshape(-1, row_count, top_count)
    )
    combined = jnp.einsum("drk,rk->rd", picked, route_weights)
    return combined.astype(jnp.bfloat16)


def on_device(
    queries,
    keys,
    values,
    lambdas,
    head_gain,
    tokens,
    route_ids,
    route_weights,
    moe_gain,
    w_gate,
    w_up,
    w_down,
):
    heads_out = attend(queries, keys, values, lambdas, head_gain)
    expert_out = experts(tokens, route_ids, route_weights, moe_gain, w_gate, w_up, w_down)
    return (heads_out, expert_out)


def solution(mesh):
    in_specs = (
        P(("grp", "ep"), "tp"),
        P(("grp", "ep"), "tp"),
        P(("grp", "ep"), "tp"),
        P("tp"),
        P(),
        P(("grp", "ep"), None),
        P(("grp", "ep"), None),
        P(("grp", "ep"), None),
        P(),
        P("ep", None, "tp"),
        P("ep", None, "tp"),
        P("ep", "tp", None),
    )
    out_specs = (P(("grp", "ep"), "tp"), P(("grp", "ep"), "tp"))
    return jax.shard_map(
        on_device, mesh=mesh, in_specs=in_specs, out_specs=out_specs, check_vma=False
    )
```

profile of v0, /device:TPU:0, one launch (start us, length us, event | category | flops | bytes accessed | tf_op | source)
XLA Modules:
  0.0 183.2 jit_solution(15858981580019613275)
XLA Ops:
  7.2 0.0 copy-start
  7.2 0.0 all-gather.2.cloned.1.call-start
  7.2 1.0 copy.40
  8.2 0.1 eq.26
  8.3 0.1 reshape.111
  8.5 0.7 broadcast_multiply_fusion
  9.2 1.2 reduce-window.6
  10.4 0.2 slice_reduce_fusion
  10.6 0.2 reduce-window.9
  10.8 0.1 add_bitcast_fusion
  10.9 0.1 copy.44
  11.0 0.1 mul.101
  11.2 2.4 %scatter_custom_fusion = s32[1024]{0:T(1024)S(1)} fusion(s32[512]{0:T(512)S(1)} %bitcast.95, s32[512]{0:T(512)S(1)} %add_select_fusion, s32[]{:T(128)} %constant.33.clone.1), kind=kCustom, calls=%fused_computation.53 | custom fusion | bytes 4100 | tf_op jit(solution)/shard_map/scatter | solution.py:67
  13.7 1.4 fusion.8
  15.1 1.4 fusion.10
  16.4 0.1 concatenate.3
  16.5 5.6 %gather_fusion = bf16[1024,1536]{1,0:T(8,128)(2,1)} fusion(bf16[257,1536]{1,0:T(8,128)(2,1)S(1)} %concatenate.3, s32[1024]{0:T(1024)S(1)} %fusion.23), kind=kCustom, calls=%fused_computation | custom fusion | bytes 6295552 | tf_op jit(solution)/shard_map/gather | solution.py:70
  22.1 1.2 constant_dynamic-slice_fusion
  23.3 26.4 %all_to_all.17 = bf16[4,256,384]{2,1,0:T(8,128)(2,1)} all-to-all(bf16[4,256,384]{2,1,0:T(8,128)(2,1)S(1)} %constant_dynamic-slice_fusion), channel_id=1, replica_groups=mesh['grp'=2,'ep'=4,'tp'=4] {'ep'}, dimensions={0} | all-to-all | bytes 1572864 | tf_op jit(solution)/shard_map/all_to_all | solution.py:78
  49.7 0.0 all-gather.2.cloned.1.call-update
  49.7 0.0 reduce-scatter.4.cloned.1.call-start
  49.8 27.7 %all-gather.2.cloned.1.call-done = bf16[4,256,1536]{2,1,0:T(8,128)(2,1)} async-done(((bf16[4,256,384]{2,1,0:T(8,128)(2,1)}), bf16[4,256,1536]{2,1,0:T(8,128)(2,1)}) %all-gather.2.cloned.1.call-update) | async-done | bytes 3145744 | tf_op jit(solution)/shard_map/all_gather | solution.py:79
  77.4 0.0 copy-start.9
  77.5 5.4 %fusion.2 = f32[4,256,768]{2,1,0:T(8,128)S(1)} fusion(bf16[4,256,1536]{2,1,0:T(8,128)(2,1)} %all-gather.2.cloned.1.call-done, bf16[1,1536,768]{2,1,0:T(8,128)(2,1)} %param.22), kind=kOutput, calls=%fused_computation.7 | convolution fusion | flops 2415919104 | bytes 8650752 | tf_op jit(solution)/shard_map/scd,df->scf/dot_general | solution.py:81
  82.8 0.0 copy-done.8
  82.8 0.0 copy-done.9
  82.8 2.9 %multiply_convert_fusion = bf16[4,256,768]{2,1,0:T(8,128)(2,1)S(1)} fusion(f32[4,256,768]{2,1,0:T(8,128)S(1)} %fusion.2, bf16[4,256,1536]{2,1,0:T(8,128)(2,1)S(1)} %copy-done.8, bf16[1,1536,768]{2,1,0:T(8,128)(2,1)S(1)} %copy-done.9), kind=kOutput, calls=%fused_computation.5 | convolution fusion | flops 2420637696 | bytes 10223616 | tf_op jit(solution)/shard_map/scd,df->scf/dot_general | solution.py:80
  85.7 0.0 copy-done
  85.8 4.0 %fusion = bf16[1536,1024]{0,1:T(8,128)(2,1)} fusion(bf16[1024,768]{1,0:T(8,128)(2,1)S(1)} %bitcast.99, bf16[1,768,1536]{2,1,0:T(8,128)(2,1)S(1)} %copy-done), kind=kOutput, calls=%fused_computation.4 | convolution fusion | flops 2417491968 | bytes 7077888 | tf_op jit(solution)/shard_map/fd,sf->ds/dot_general | solution.py:85
  89.8 4.6 %copy.49 = bf16[1536,1024]{1,0:T(8,128)(2,1)} copy(bf16[1536,1024]{0,1:T(8,128)(2,1)} %fusion) | data formatting | bytes 6291456
  94.4 0.0 copy-start.4
  94.4 0.0 copy-start.5
  94.4 0.0 reduce-scatter.4.cloned.1.call-update
  94.5 0.0 copy-start.2
  94.5 0.1 reduce_sum.43
  94.6 0.1 copy.42
  94.7 0.4 copy-done.4
  95.1 0.8 copy.43
  95.9 0.0 copy-done.5
  95.9 0.8 copy.47
  96.7 0.0 copy-done.1
  96.7 13.9 %all_gather.9 = bf16[512,256]{1,0:T(8,128)(2,1)S(1)} all-gather(bf16[128,256]{1,0:T(8,128)(2,1)S(1)} %copy-done.1), channel_id=1, replica_groups=mesh['grp'=2,'ep'=4,'tp'=4] {'ep'}, dimensions={0}, use_global_device_ids=true | all-gather | bytes 327680 | tf_op jit(solution)/shard_map/all_gather | solution.py:15
  110.6 0.1 copy.37
  110.8 0.0 copy-done.3
  110.8 0.1 copy.36
  110.9 1.3 fusion.30
  112.2 20.3 %reduce-scatter.4.cloned.1.call-done = bf16[384,1024]{1,0:T(8,128)(2,1)} async-done(((bf16[1536,1024]{1,0:T(8,128)(2,1)}), bf16[384,1024]{1,0:T(8,128)(2,1)}) %reduce-scatter.4.cloned.1.call-update) | async-done | bytes 786448
  132.5 2.3 %copy.50 = bf16[384,1024]{0,1:T(8,128)(2,1)} copy(bf16[384,1024]{1,0:T(8,128)(2,1)} %reduce-scatter.4.cloned.1.call-done) | data formatting | bytes 1572864
  134.8 4.7 %all-to-all-start.1 = ((bf16[384,4,256]{0,2,1:T(8,128)(2,1)}), bf16[384,4,256]{0,2,1:T(8,128)(2,1)S(1)}, u32[]{:S(2)}, u32[]{:S(2)}) async-start(bf16[384,4,256]{0,2,1:T(8,128)(2,1)} %bitcast.87), calls=%async_computation.1 | async-start | bytes 1572864 | tf_op jit(solution)/shard_map/all_to_all | solution.py:92
  139.5 0.0 copy-done.2
  139.5 27.2 %all_gather.10 = bf16[512,256]{1,0:T(8,128)(2,1)S(1)} all-gather(bf16[128,256]{1,0:T(8,128)(2,1)S(1)} %copy-done.2), channel_id=1, replica_groups=mesh['grp'=2,'ep'=4,'tp'=4] {'ep'}, dimensions={0}, use_global_device_ids=true | all-gather | bytes 327680 | tf_op jit(solution)/shard_map/all_gather | solution.py:16
  166.7 0.9 copy.38
  167.6 1.5 fusion.11
  169.1 1.7 convolution_divide_fusion
  170.9 0.0 copy-done.6
  170.9 0.1 multiply_reduce_fusion
  171.0 0.0 copy-done.7
  171.0 0.1 multiply_convert_fusion.1
  171.1 0.7 copy.45
  171.8 0.0 all-to-all-done.1
  171.8 1.9 %gather_fusion.1 = bf16[512,384]{1,0:T(8,128)(2,1)S(1)} fusion(bf16[384,1024]{0,1:T(8,128)(2,1)S(1)} %bitcast.85, s32[1024]{0:T(1024)S(1)} %pad_clamp_fusion), kind=kCustom, calls=%fused_computation.1 | custom fusion | bytes 788480 | tf_op jit(solution)/shard_map/jit(_take)/gather | solution.py:94
  173.8 0.1 gather.11
  173.9 1.7 fusion.15
  175.7 0.7 copy.55
  (15 shorter events, 0.1 us)
Async XLA Ops:
  7.2 78.6 %copy-start = (bf16[1,768,1536]{2,1,0:T(8,128)(2,1)S(1)}, bf16[1,768,1536]{2,1,0:T(8,128)(2,1)}, u32[]{:S(2)}) copy-start(bf16[1,768,1536]{2,1,0:T(8,128)(2,1)} %param.23) | copy-start | bytes 7077892
  7.2 70.3 %all-gather.2.cloned.1.call-start = ((), (), s32[]{:S(2)}) async-start(), calls=%async_computation.3 | async-start | bytes 3932160 | tf_op jit(solution)/shard_map/all_gather | solution.py:79
  49.7 82.8 %reduce-scatter.4.cloned.1.call-start = ((), (), s32[]{:S(2)}) async-start(), calls=%async_computation.4 | async-start | bytes 3932160
  77.4 5.4 %copy-start.8 = (bf16[4,256,1536]{2,1,0:T(8,128)(2,1)S(1)}, bf16[4,256,1536]{2,1,0:T(8,128)(2,1)}, u32[]{:S(2)}) copy-start(bf16[4,256,1536]{2,1,0:T(8,128)(2,1)} %all-gather.2.cloned.1.call-done) | copy-start | bytes 9437188
  77.4 5.4 %copy-start.9 = (bf16[1,1536,768]{2,1,0:T(8,128)(2,1)S(1)}, bf16[1,1536,768]{2,1,0:T(8,128)(2,1)}, u32[]{:S(2)}) copy-start(bf16[1,1536,768]{2,1,0:T(8,128)(2,1)} %param.21) | copy-start | bytes 7077892
  94.4 0.7 copy-start.4
  94.4 1.4 copy-start.5
  94.4 2.3 %copy-start.1 = (bf16[128,256]{1,0:T(8,128)(2,1)S(1)}, bf16[128,256]{1,0:T(8,128)(2,1)}, u32[]{:S(2)}) copy-start(bf16[128,256]{1,0:T(8,128)(2,1)} %param.13) | copy-start | bytes 196612
  94.4 16.4 %copy-start.3 = (bf16[128,256]{1,0:T(8,128)(2,1)S(1)}, bf16[128,256]{1,0:T(8,128)(2,1)}, u32[]{:S(2)}) copy-start(bf16[128,256]{1,0:T(8,128)(2,1)} %param.12) | copy-start | bytes 196612
  94.5 45.1 %copy-start.2 = (bf16[128,256]{1,0:T(8,128)(2,1)S(1)}, bf16[128,256]{1,0:T(8,128)(2,1)}, u32[]{:S(2)}) copy-start(bf16[128,256]{1,0:T(8,128)(2,1)} %param.14) | copy-start | bytes 196612
  112.2 58.6 %copy-start.6 = (f32[2]{0:T(128)S(1)}, f32[2]{0:T(128)}, u32[]{:S(2)}) copy-start(f32[2]{0:T(128)} %param.15) | copy-start | bytes 28
  134.8 36.2 %copy-start.7 = (f32[128]{0:T(128)S(1)}, f32[128]{0:T(128)}, u32[]{:S(2)}) copy-start(f32[128]{0:T(128)} %param.16) | copy-start | bytes 1540
  134.8 37.1 %all-to-all-start.1 = ((bf16[384,4,256]{0,2,1:T(8,128)(2,1)}), bf16[384,4,256]{0,2,1:T(8,128)(2,1)S(1)}, u32[]{:S(2)}, u32[]{:S(2)}) async-start(bf16[384,4,256]{0,2,1:T(8,128)(2,1)} %bitcast.87), calls=%async_computation.1 | async-start | bytes 1572864 | tf_op jit(solution)/shard_map/all_to_all | solution.py:92
Sparse Core Ops, SparseCore 0:
  49.8 27.5 all-gather.1
  94.6 37.8 reduce-scatter.3
where the time goes:
time: 184 us; the launch traced here: 183 us
  blocking collectives  67.5 us (37%)
  waiting for transfers between devices  48 us (26%)
  local copies, waits for them, and re-layouts  24.9 us (14%)
  matrix products  17 us (9%)
  between operations  14.3 us (8%)
  other arithmetic  6.72 us (4%)
  starting transfers between devices  4.81 us (3%)
    all_gather x1, waiting for transfers between devices, experts(): piece = lax.all_gather(arrived, 'tp', axis=2, tiled=True)  27.7 us
    all_gather x1, blocking collectives, attend(): value_piece = lax.all_gather(values, 'ep', axis=0, tiled=True)  27.2 us
    all_to_all x1, blocking collectives, experts(): lax.all_to_all(own_columns, 'ep', split_axis=0, concat_axis=0, tiled=True)  26.4 us
    unnamed x3, waiting for transfers between devices  20.3 us
    all_gather x1, blocking collectives, attend(): key_piece = lax.all_gather(keys, 'ep', axis=0, tiled=True)  13.9 us
    unnamed x26, local copies, waits for them, and re-layouts  10 us
    gather x1, local copies, waits for them, and re-layouts, experts(): outgoing = padded[owners].reshape(expert_count, capacity, width)  5.61 us
    dot_general x1, matrix products, experts(): jnp.einsum('scd,df->scf', piece, up_mat, preferred_element_type=jnp.float32)  5.36 us
  transfers between devices with their start and end apart: 3, of which 2 were waited for; matrix products, arithmetic and copies ran while one was open for 5% of the time, Pallas kernels for 0%

commit v1 on v0

--- a/solution.py
+++ b/solution.py
@@ -76,7 +76,10 @@
         outgoing, lax.axis_index("tp") * slice_width, slice_width, 2
     )
     arrived = lax.all_to_all(own_columns, "ep", split_axis=0, concat_axis=0, tiled=True)
-    piece = lax.all_gather(arrived, "tp", axis=2, tiled=True)
+    devices = lax.axis_size("tp")
+    pieces = jnp.stack([arrived for _ in range(devices)])
+    pieces = lax.all_to_all(pieces, "tp", split_axis=0, concat_axis=0)
+    piece = jnp.concatenate(pieces, axis=2)
     gate = jnp.einsum("scd,df->scf", piece, gate_mat, preferred_element_type=jnp.float32)
     upward = jnp.einsum("scd,df->scf", piece, up_mat, preferred_element_type=jnp.float32)
     hidden = (jax.nn.silu(gate) * upward).astype(jnp.bfloat16)

time: 184 us -> 193 us (1.049)
  blocking collectives: 67.5 us -> 107 us
  waiting for transfers between devices: 48 us -> 17.9 us
  matrix products: 17 us -> 14.3 us
  local copies, waits for them, and re-layouts: 24.9 us -> 27 us
    all_to_all x0 -> x1, blocking collectives: none -> 39.5 us  [experts(): pieces = lax.all_to_all(pieces, 'tp', split_axis=0, concat_axis=0)]
    all_gather x1 -> x0, waiting for transfers between devices: 27.7 us -> none  [experts(): piece = lax.all_gather(arrived, 'tp', axis=2, tiled=True)]
    dot_general x1, matrix products: 5.36 us -> 2.59 us  [experts(): jnp.einsum('scd,df->scf', piece, up_mat, preferred_element_type=jnp.float32)]
    unnamed x3 -> x2, waiting for transfers between devices: 20.3 us -> 17.9 us
  transfers between devices with their start and end apart: 3 -> 2, of which waited for: 2 -> 1; matrix products, arithmetic and copies ran while one was open for 5% -> 4% of each run, Pallas kernels for 0% -> 0%
where the time goes in v1:
time: 193 us; the launch traced here: 192 us
  blocking collectives  107 us (55%)
  local copies, waits for them, and re-layouts  27 us (14%)
  waiting for transfers between devices  17.9 us (9%)
  matrix products  14.3 us (7%)
  between operations  14.3 us (7%)
  other arithmetic  6.72 us (3%)
  starting transfers between devices  4.78 us (2%)
    all_to_all x1, blocking collectives, experts(): pieces = lax.all_to_all(pieces, 'tp', split_axis=0, concat_axis=0)  39.5 us
    all_gather x1, blocking collectives, attend(): value_piece = lax.all_gather(values, 'ep', axis=0, tiled=True)  27.2 us
    all_to_all x1, blocking collectives, experts(): lax.all_to_all(own_columns, 'ep', split_axis=0, concat_axis=0, tiled=True)  26.3 us
    unnamed x2, waiting for transfers between devices  17.9 us
    all_gather x1, blocking collectives, attend(): key_piece = lax.all_gather(keys, 'ep', axis=0, tiled=True)  14.4 us
    unnamed x26, local copies, waits for them, and re-layouts  11.3 us
    gather x1, local copies, waits for them, and re-layouts, experts(): outgoing = padded[owners].reshape(expert_count, capacity, width)  5.61 us
    all_to_all x1, starting transfers between devices, experts(): back = lax.all_to_all(summed, 'ep', split_axis=1, concat_axis=1, tiled=True)  4.74 us
  transfers between devices with their start and end apart: 2, of which 1 were waited for; matrix products, arithmetic and copies ran while one was open for 4% of the time, Pallas kernels for 0%

profile of v1, /device:TPU:0, one launch (start us, length us, event | category | flops | bytes accessed | tf_op | source)
XLA Modules:
  0.0 192.3 jit_solution(18257608637831585549)
XLA Ops:
  7.2 0.0 copy-start
  7.2 0.0 reduce-scatter.4.cloned.1.call-start
  7.2 1.0 copy.41
  8.2 0.1 eq.26
  8.3 0.1 reshape.119
  8.5 0.7 broadcast_multiply_fusion
  9.2 1.2 reduce-window.6
  10.4 0.2 slice_reduce_fusion
  10.6 0.2 reduce-window.9
  10.8 0.1 add_bitcast_fusion
  10.9 0.1 copy.45
  11.0 0.1 mul.101
  11.2 2.4 %scatter_custom_fusion = s32[1024]{0:T(1024)S(1)} fusion(s32[512]{0:T(512)S(1)} %bitcast.101, s32[512]{0:T(512)S(1)} %add_select_fusion, s32[]{:T(128)} %constant.33.clone.1), kind=kCustom, calls=%fused_computation.53 | custom fusion | bytes 4100 | tf_op jit(solution)/shard_map/scatter | solution.py:67
  13.7 1.4 fusion.8
  15.1 1.4 fusion.10
  16.4 0.1 concatenate.3
  16.5 5.6 %gather_fusion = bf16[1024,1536]{1,0:T(8,128)(2,1)} fusion(bf16[257,1536]{1,0:T(8,128)(2,1)S(1)} %concatenate.3, s32[1024]{0:T(1024)S(1)} %fusion.23), kind=kCustom, calls=%fused_computation | custom fusion | bytes 6295552 | tf_op jit(solution)/shard_map/gather | solution.py:70
  22.1 1.2 constant_dynamic-slice_fusion
  23.3 26.3 %all_to_all.22 = bf16[4,256,384]{2,1,0:T(8,128)(2,1)S(1)} all-to-all(bf16[4,256,384]{2,1,0:T(8,128)(2,1)S(1)} %constant_dynamic-slice_fusion), channel_id=1, replica_groups=mesh['grp'=2,'ep'=4,'tp'=4] {'ep'}, dimensions={0} | all-to-all | bytes 1572864 | tf_op jit(solution)/shard_map/all_to_all | solution.py:78
  49.6 0.4 stack.2
  50.0 39.5 %all_to_all.23 = bf16[4,4,256,384]{3,2,1,0:T(8,128)(2,1)S(1)} all-to-all(bf16[4,4,256,384]{3,2,1,0:T(8,128)(2,1)S(1)} %stack.2), channel_id=1, replica_groups=mesh['grp'=2,'ep'=4,'tp'=4] {'tp'}, dimensions={0} | all-to-all | bytes 6291456 | tf_op jit(solution)/shard_map/all_to_all | solution.py:81
  89.5 0.0 copy-start.8
  89.5 0.4 copy.54
  89.9 1.3 copy-done.8
  91.1 0.0 copy-start.9
  91.1 2.6 %fusion.2 = f32[4,256,768]{2,1,0:T(8,128)S(1)} fusion(bf16[4,256,1536]{2,1,0:T(8,128)(2,1)S(1)} %bitcast.91, bf16[1,1536,768]{2,1,0:T(8,128)(2,1)S(1)} %copy-done.8), kind=kOutput, calls=%fused_computation.7 | convolution fusion | flops 2415919104 | bytes 8650752 | tf_op jit(solution)/shard_map/scd,df->scf/dot_general | solution.py:84
  93.7 0.0 copy-done.9
  93.8 2.9 %multiply_convert_fusion = bf16[4,256,768]{2,1,0:T(8,128)(2,1)S(1)} fusion(f32[4,256,768]{2,1,0:T(8,128)S(1)} %fusion.2, bf16[4,256,1536]{2,1,0:T(8,128)(2,1)S(1)} %bitcast.92, bf16[1,1536,768]{2,1,0:T(8,128)(2,1)S(1)} %copy-done.9), kind=kOutput, calls=%fused_computation.5 | convolution fusion | flops 2420637696 | bytes 10223616 | tf_op jit(solution)/shard_map/scd,df->scf/dot_general | solution.py:83
  96.7 0.0 copy-done
  96.7 4.0 %fusion = bf16[1536,1024]{0,1:T(8,128)(2,1)} fusion(bf16[1024,768]{1,0:T(8,128)(2,1)S(1)} %bitcast.105, bf16[1,768,1536]{2,1,0:T(8,128)(2,1)S(1)} %copy-done), kind=kOutput, calls=%fused_computation.4 | convolution fusion | flops 2417491968 | bytes 7077888 | tf_op jit(solution)/shard_map/fd,sf->ds/dot_general | solution.py:88
  100.7 4.6 %copy.51 = bf16[1536,1024]{1,0:T(8,128)(2,1)} copy(bf16[1536,1024]{0,1:T(8,128)(2,1)} %fusion) | data formatting | bytes 6291456
  105.3 0.0 copy-start.4
  105.3 0.0 reduce-scatter.4.cloned.1.call-update
  105.4 0.0 copy-start.2
  105.4 0.1 reduce_sum.43
  105.5 0.1 copy.43
  105.6 0.4 copy-done.4
  106.0 0.8 copy.44
  106.8 0.0 copy-done.5
  106.8 0.8 copy.49
  107.6 0.0 copy-done.1
  107.6 14.4 %all_gather.6 = bf16[512,256]{1,0:T(8,128)(2,1)S(1)} all-gather(bf16[128,256]{1,0:T(8,128)(2,1)S(1)} %copy-done.1), channel_id=1, replica_groups=mesh['grp'=2,'ep'=4,'tp'=4] {'ep'}, dimensions={0}, use_global_device_ids=true | all-gather | bytes 327680 | tf_op jit(solution)/shard_map/all_gather | solution.py:15
  122.0 0.1 copy.38
  122.2 0.0 copy-done.3
  122.2 0.1 copy.37
  122.3 1.3 fusion.30
  123.7 17.9 %reduce-scatter.4.cloned.1.call-done = bf16[384,1024]{1,0:T(8,128)(2,1)} async-done(((bf16[1536,1024]{1,0:T(8,128)(2,1)}), bf16[384,1024]{1,0:T(8,128)(2,1)}) %reduce-scatter.4.cloned.1.call-update) | async-done | bytes 786448
  141.6 2.3 %copy.52 = bf16[384,1024]{0,1:T(8,128)(2,1)} copy(bf16[384,1024]{1,0:T(8,128)(2,1)} %reduce-scatter.4.cloned.1.call-done) | data formatting | bytes 1572864
  143.9 4.7 %all-to-all-start.2 = ((bf16[384,4,256]{0,2,1:T(8,128)(2,1)}), bf16[384,4,256]{0,2,1:T(8,128)(2,1)S(1)}, u32[]{:S(2)}, u32[]{:S(2)}) async-start(bf16[384,4,256]{0,2,1:T(8,128)(2,1)} %bitcast.93), calls=%async_computation.2 | async-start | bytes 1572864 | tf_op jit(solution)/shard_map/all_to_all | solution.py:95
  148.6 0.0 copy-done.2
  148.6 27.2 %all_gather.7 = bf16[512,256]{1,0:T(8,128)(2,1)S(1)} all-gather(bf16[128,256]{1,0:T(8,128)(2,1)S(1)} %copy-done.2), channel_id=1, replica_groups=mesh['grp'=2,'ep'=4,'tp'=4] {'ep'}, dimensions={0}, use_global_device_ids=true | all-gather | bytes 327680 | tf_op jit(solution)/shard_map/all_gather | solution.py:16
  175.8 0.9 copy.39
  176.7 1.5 fusion.11
  178.2 1.7 convolution_divide_fusion
  179.9 0.0 copy-done.6
  180.0 0.1 multiply_reduce_fusion
  180.1 0.0 copy-done.7
  180.1 0.1 multiply_convert_fusion.1
  180.2 0.7 copy.47
  180.9 0.0 all-to-all-done.2
  180.9 1.9 %gather_fusion.1 = bf16[512,384]{1,0:T(8,128)(2,1)S(1)} fusion(bf16[384,1024]{0,1:T(8,128)(2,1)S(1)} %bitcast.88, s32[1024]{0:T(1024)S(1)} %pad_clamp_fusion), kind=kCustom, calls=%fused_computation.1 | custom fusion | bytes 788480 | tf_op jit(solution)/shard_map/jit(_take)/gather | solution.py:97
  182.9 0.1 gather.11
  183.0 1.7 fusion.15
  184.8 0.7 copy.58
  (15 shorter events, 0.1 us)
Async XLA Ops:
  7.2 89.5 %copy-start = (bf16[1,768,1536]{2,1,0:T(8,128)(2,1)S(1)}, bf16[1,768,1536]{2,1,0:T(8,128)(2,1)}, u32[]{:S(2)}) copy-start(bf16[1,768,1536]{2,1,0:T(8,128)(2,1)} %param.23) | copy-start | bytes 7077892
  7.2 134.4 %reduce-scatter.4.cloned.1.call-start = ((), (), s32[]{:S(2)}) async-start(), calls=%async_computation.4 | async-start | bytes 3932160
  89.5 1.7 copy-start.8
  91.1 2.6 %copy-start.9 = (bf16[1,1536,768]{2,1,0:T(8,128)(2,1)S(1)}, bf16[1,1536,768]{2,1,0:T(8,128)(2,1)}, u32[]{:S(2)}) copy-start(bf16[1,1536,768]{2,1,0:T(8,128)(2,1)} %param.21) | copy-start | bytes 7077892
  105.3 0.7 copy-start.4
  105.3 1.4 copy-start.5
  105.3 2.3 %copy-start.1 = (bf16[128,256]{1,0:T(8,128)(2,1)S(1)}, bf16[128,256]{1,0:T(8,128)(2,1)}, u32[]{:S(2)}) copy-start(bf16[128,256]{1,0:T(8,128)(2,1)} %param.13) | copy-start | bytes 196612
  105.3 16.9 %copy-start.3 = (bf16[128,256]{1,0:T(8,128)(2,1)S(1)}, bf16[128,256]{1,0:T(8,128)(2,1)}, u32[]{:S(2)}) copy-start(bf16[128,256]{1,0:T(8,128)(2,1)} %param.12) | copy-start | bytes 196612
  105.4 43.2 %copy-start.2 = (bf16[128,256]{1,0:T(8,128)(2,1)S(1)}, bf16[128,256]{1,0:T(8,128)(2,1)}, u32[]{:S(2)}) copy-start(bf16[128,256]{1,0:T(8,128)(2,1)} %param.14) | copy-start | bytes 196612
  123.7 56.3 %copy-start.6 = (f32[2]{0:T(128)S(1)}, f32[2]{0:T(128)}, u32[]{:S(2)}) copy-start(f32[2]{0:T(128)} %param.15) | copy-start | bytes 28
  143.9 36.2 %copy-start.7 = (f32[128]{0:T(128)S(1)}, f32[128]{0:T(128)}, u32[]{:S(2)}) copy-start(f32[128]{0:T(128)} %param.16) | copy-start | bytes 1540
  143.9 37.1 %all-to-all-start.2 = ((bf16[384,4,256]{0,2,1:T(8,128)(2,1)}), bf16[384,4,256]{0,2,1:T(8,128)(2,1)S(1)}, u32[]{:S(2)}, u32[]{:S(2)}) async-start(bf16[384,4,256]{0,2,1:T(8,128)(2,1)} %bitcast.93), calls=%async_computation.2 | async-start | bytes 1572864 | tf_op jit(solution)/shard_map/all_to_all | solution.py:95
Sparse Core Ops, SparseCore 0:
  105.5 36.0 reduce-scatter.3
